TPU v7x, 32 devices: a whole 2x2x4 slice. The times are simulated.
32 devices in a mesh: kv: 8 (over z, y), tp: 4 (over x, core).
Axes of the slice: x: 2, y: 2, z: 4, core: 2. Of those that a mesh axis runs over, the one named last changes fastest.
Arguments:
- queries: bfloat16 [2048, 3072], P('kv', 'tp'), may hold values from -6 to 6
- key_vectors: bfloat16 [2048, 512], P('kv', 'tp'), may hold values from -6 to 6
- value_vectors: bfloat16 [2048, 512], P('kv', 'tp'), may hold values from -6 to 6
- log_sums: float32 [2048, 48], P('kv', 'tp'), may hold values from 4.5 to 6.5
- out_grad: bfloat16 [2048, 3072], P('kv', 'tp'), may hold values from -48 to 48
- layer_input: bfloat16 [2048, 3072], P('kv', 'tp'), may hold values from -0.29882812 to 0.29882812
- chosen: int32 [32, 16], P('kv'), may hold values from -1 to 55, as said below
Outputs:
- query_grad: bfloat16 [2048, 3072], P('kv', 'tp')
- key_grad: bfloat16 [2048, 512], P('kv', 'tp')
- value_grad: bfloat16 [2048, 512], P('kv', 'tp')
- weight_grad: float32 [3072, 512], P('kv', 'tp')
Inputs may be any that keep to these rules, and one draw needn't show every extreme that they name: `chosen`: each entry is -1 or the number c of a block of 32 positions (c * 32 to c * 32 + 31) that lies wholly within an earlier index of kv than its query block. The numbers of one row differ, and all query blocks held by one index of kv together take at most one block from each other index.
All inputs are finite; a program needn't handle non-finite values.
Results may differ from a plain program's by a relative error of at most 0.0061.
Values may be sent and summed in bfloat16 or wider, within the bound.
No kernel may reach another device: no remote copies, remote signals or barrier semaphores. Data moves between devices by JAX's collectives and lax.ppermute only.
A program may use at most 64 MiB of HBM per device.

v0:
```python
import jax
import jax.numpy as jnp
from jax import lax
from jax.sharding import PartitionSpec as P

HEAD = 64
KB = 32
QB = 64
NSEL = 16


def per_device(queries, key_vectors, value_vectors, log_sums, out_grad, layer_input, chosen):
    axis_count = lax.axis_size("kv")
    own_index = lax.axis_index("kv")
    span_rows = queries.shape[0]
    kv_local = key_vectors.shape[1] // HEAD
    group_size = queries.shape[1] // key_vectors.shape[1]
    blocks_here = span_rows // KB
    query_blocks = span_rows // QB
    score_scale = HEAD ** (-0.5)
    half_width = kv_local * HEAD
    pair_width = 2 * half_width
    paired = jnp.concatenate([key_vectors, value_vectors], axis=1)
    owners = jnp.arange(axis_count, dtype=jnp.int32)
    usable = chosen >= 0
    owner_of = jnp.where(usable, chosen // blocks_here, -1)
    within = chosen - chosen // blocks_here * blocks_here
    matched = owner_of[:, :, None] == owners[None, None, :]
    wanted = jnp.max(jnp.where(matched, within[:, :, None], -1), axis=(0, 1))
    incoming = lax.all_to_all(wanted[:, None], "kv", split_axis=0, concat_axis=0, tiled=True)[:, 0]
    blocks = paired.reshape(blocks_here, KB, pair_width)
    outgoing = jnp.where(
        (incoming >= 0)[:, None, None],
        blocks[jnp.maximum(incoming, 0)],
        jnp.zeros((), paired.dtype),
    )
    fetched = lax.all_to_all(outgoing, "kv", split_axis=0, concat_axis=0, tiled=True)
    query_parts = queries.reshape(query_blocks, QB, kv_local, group_size, HEAD)
    grad_parts = out_grad.reshape(query_blocks, QB, kv_local, group_size, HEAD)
    sum_parts = log_sums.reshape(query_blocks, QB, kv_local, group_size)
    slot_owner = jnp.clip(owner_of, 0, axis_count - 1)
    key_own = key_vectors.reshape(span_rows, kv_local, HEAD)
    value_own = value_vectors.reshape(span_rows, kv_local, HEAD)
    key_pos = own_index * span_rows + jnp.arange(span_rows, dtype=jnp.int32)

    def one_block(packed):
        query_part, grad_part, sum_part, slot_part, usable_part, block_index = packed
        selected = fetched[slot_part].reshape(NSEL * KB, 2, kv_local, HEAD)
        key_sel = selected[:, 0]
        value_sel = selected[:, 1]
        keep_key = jnp.repeat(usable_part, KB)
        query_pos = own_index * span_rows + block_index * QB + jnp.arange(QB, dtype=jnp.int32)
        causal = key_pos[None, :] <= query_pos[:, None]
        score_sel = (
            jnp.einsum("qhgd,khd->qhgk", query_part, key_sel, preferred_element_type=jnp.float32)
            * score_scale
        )
        score_own = (
            jnp.einsum("qhgd,khd->qhgk", query_part, key_own, preferred_element_type=jnp.float32)
            * score_scale
        )
        weight_sel = jnp.where(
            keep_key[None, None, None, :], jnp.exp(score_sel - sum_part[..., None]), 0.0
        )
        weight_own = jnp.where(
            causal[:, None, None, :], jnp.exp(score_own - sum_part[..., None]), 0.0
        )
        round_sel = weight_sel.astype(jnp.bfloat16)
        round_own = weight_own.astype(jnp.bfloat16)
        output = jnp.einsum(
            "qhgk,khd->qhgd", round_sel, value_sel, preferred_element_type=jnp.float32
        )
        output = output + jnp.einsum(
            "qhgk,khd->qhgd", round_own, value_own, preferred_element_type=jnp.float32
        )
        row_delta = jnp.sum(grad_part.astype(jnp.float32) * output, axis=-1)
        prod_sel = jnp.einsum(
            "qhgd,khd->qhgk", grad_part, value_sel, preferred_element_type=jnp.float32
        )
        prod_own = jnp.einsum(
            "qhgd,khd->qhgk", grad_part, value_own, preferred_element_type=jnp.float32
        )
        slope_sel = (weight_sel * (prod_sel - row_delta[..., None])).astype(jnp.bfloat16)
        slope_own = (weight_own * (prod_own - row_delta[..., None])).astype(jnp.bfloat16)
        query_total = jnp.einsum(
            "qhgk,khd->qhgd", slope_sel, key_sel, preferred_element_type=jnp.float32
        )
        query_total = query_total + jnp.einsum(
            "qhgk,khd->qhgd", slope_own, key_own, preferred_element_type=jnp.float32
        )
        query_out = (query_total * score_scale).astype(jnp.bfloat16)
        key_sel_grad = (
            jnp.einsum("qhgk,qhgd->khd", slope_sel, query_part, preferred_element_type=jnp.float32)
            * score_scale
        )
        value_sel_grad = jnp.einsum(
            "qhgk,qhgd->khd", round_sel, grad_part, preferred_element_type=jnp.float32
        )
        key_own_grad = (
            jnp.einsum("qhgk,qhgd->khd", slope_own, query_part, preferred_element_type=jnp.float32)
            * score_scale
        )
        value_own_grad = jnp.einsum(
            "qhgk,qhgd->khd", round_own, grad_part, preferred_element_type=jnp.float32
        )
        sel_pair = jnp.concatenate(
            [
                key_sel_grad.reshape(NSEL, KB, half_width),
                value_sel_grad.reshape(NSEL, KB, half_width),
            ],
            axis=2,
        )
        own_pair = jnp.concatenate(
            [
                key_own_grad.reshape(span_rows, half_width),
                value_own_grad.reshape(span_rows, half_width),
            ],
            axis=1,
        )
        return (query_out, sel_pair, own_pair)

    block_ids = jnp.arange(query_blocks, dtype=jnp.int32)
    query_outs, sel_pairs, own_pairs = lax.map(
        one_block, (query_parts, grad_parts, sum_parts, slot_owner, usable, block_ids)
    )
    onehot = ((slot_owner[:, :, None] == owners[None, None, :]) & usable[:, :, None]).astype(
        jnp.float32
    )
    onehot = onehot.reshape(query_blocks * NSEL, axis_count)
    per_owner = jnp.einsum(
        "so,sr->or",
        onehot,
        sel_pairs.reshape(query_blocks * NSEL, KB * pair_width),
        precision=lax.Precision.HIGHEST,
    )
    returned = lax.all_to_all(
        per_owner.reshape(axis_count, KB, pair_width), "kv", split_axis=0, concat_axis=0, tiled=True
    )
    placing = (incoming[None, :] == jnp.arange(blocks_here, dtype=jnp.int32)[:, None]).astype(
        jnp.float32
    )
    landed = jnp.einsum(
        "bs,sr->br",
        placing,
        returned.reshape(axis_count, KB * pair_width),
        precision=lax.Precision.HIGHEST,
    )
    totals = jnp.sum(own_pairs, axis=0) + landed.reshape(span_rows, pair_width)
    key_grad = totals[:, :half_width].astype(jnp.bfloat16)
    value_grad = totals[:, half_width:].astype(jnp.bfloat16)
    full_input = lax.all_gather(layer_input, "tp", axis=1, tiled=True)
    weight_grad = lax.psum_scatter(
        lax.dot_general(
            full_input, key_grad, (((0,), (0,)), ((), ())), preferred_element_type=jnp.float32
        ),
        "kv",
        scatter_dimension=0,
        tiled=True,
    )
    return (query_outs.reshape(span_rows, queries.shape[1]), key_grad, value_grad, weight_grad)


def solution(mesh):
    placed = (
        P("kv", "tp"),
        P("kv", "tp"),
        P("kv", "tp"),
        P("kv", "tp"),
        P("kv", "tp"),
        P("kv", "tp"),
        P("kv", None),
    )
    return jax.shard_map(
        per_device,
        mesh=mesh,
        in_specs=placed,
        out_specs=(P("kv", "tp"), P("kv", "tp"), P("kv", "tp"), P("kv", "tp")),
        check_vma=False,
    )
```

profile of v0, /device:TPU:0, one launch (start us, length us, event | category | flops | bytes accessed | tf_op | source)
XLA Modules:
  0.0 224.7 jit_solution(12152546866315410712)
XLA Ops:
  7.2 1.3 broadcast_clamp_fusion
  9.3 7.3 %all-to-all-start = ((s32[8,1,1]{2,1,0:T(1,128)}), s32[8,1,1]{2,1,0:T(1,128)S(1)}, u32[]{:S(2)}, u32[]{:S(2)}) async-start(s32[8,1,1]{2,1,0:T(1,128)} %copy.110), calls=%async_computation | async-start | bytes 8192 | tf_op jit(solution)/shard_map/all_to_all | solution.py:30
  17.5 5.5 %all-to-all-done = s32[8,1,1]{2,1,0:T(1,128)S(1)} async-done(((s32[8,1,1]{2,1,0:T(1,128)}), s32[8,1,1]{2,1,0:T(1,128)S(1)}, u32[]{:S(2)}, u32[]{:S(2)}) %all-to-all-start) | async-done | bytes 64 | tf_op jit(solution)/shard_map/all_to_all | solution.py:30
  24.9 3.4 %all-to-all-start.1 = ((bf16[8,32,256]{2,1,0:T(8,128)(2,1)}), bf16[8,32,256]{2,1,0:T(8,128)(2,1)S(1)}, u32[]{:S(2)}, u32[]{:S(2)}) async-start(bf16[8,32,256]{2,1,0:T(8,128)(2,1)} %broadcast_select_fusion), calls=%async_computation.1 | async-start | bytes 262144 | tf_op jit(solution)/shard_map/all_to_all | solution.py:37
  29.1 1.6 copy.113
  35.0 1.2 and.19
  36.9 93.2 %while.18 = (s32[]{:T(128)}, bf16[4,64,2,6,64]{1,4,3,2,0:T(8,128)(2,1)}, f32[4,16,32,256]{3,2,1,0:T(8,128)}, f32[4,256,256]{1,2,0:T(8,128)}, s32[4,16]{1,0:T(4,1...) while((s32[]{:T(128)}, ...), condition=%wide.region_3.4_spmd.clone.clone, body=%wide.region_1.3_spmd.clone.clone.sunk | while | flops 458359424 | bytes 25241412 | solution.py:123
  39.2 1.4 fusion.153
  42.5 1.2 fusion.154
  43.8 1.3 fusion.155
  45.1 1.3 fusion.156
  46.3 1.2 fusion.159
  48.6 2.0 reshape.226
  50.6 1.2 convolution_bitcast_fusion.14
  53.7 1.2 fusion.157
  58.5 1.8 fusion.158
  62.5 1.4 fusion.153
  65.8 1.2 fusion.154
  67.0 1.3 fusion.155
  68.3 1.3 fusion.156
  69.6 1.2 fusion.159
  71.9 2.0 reshape.226
  73.9 1.2 convolution_bitcast_fusion.14
  76.9 1.2 fusion.157
  81.7 1.8 fusion.158
  85.8 1.4 fusion.153
  89.0 1.2 fusion.154
  90.3 1.3 fusion.155
  91.6 1.3 fusion.156
  92.9 1.2 fusion.159
  95.1 2.0 reshape.226
  97.2 1.2 convolution_bitcast_fusion.14
  100.2 1.2 fusion.157
  105.0 1.8 fusion.158
  109.1 1.4 fusion.153
  113.6 1.3 fusion.155
  114.9 1.3 fusion.156
  116.2 1.2 fusion.159
  118.4 2.0 reshape.226
  123.5 1.2 fusion.157
  128.3 1.8 fusion.158
  130.1 3.5 %fusion.66 = f32[8,32,256]{2,0,1:T(8,128)S(1)} fusion(s32[64]{0:T(128)} %eq.51, pred[64]{0:T(512)(128)(4,1)} %and.19, f32[8,8,32,256]{3,2,1,0:T(8,128)} %bitcast.274), kind=kOutput, calls=%fused_computation.90 | convolution fusion | flops 50332672 | bytes 2359616 | tf_op jit(solution)/shard_map/so,sr->or/dot_general | solution.py:130
  134.5 5.9 %all-to-all-start.2 = ((f32[8,32,256]{2,1,0:T(8,128)}), f32[8,32,256]{2,1,0:T(8,128)S(1)}, u32[]{:S(2)}, u32[]{:S(2)}) async-start(f32[8,32,256]{2,1,0:T(8,128)} %copy.120), calls=%async_computation.2 | async-start | bytes 524288 | tf_op jit(solution)/shard_map/all_to_all | solution.py:136
  140.7 7.9 %all-to-all-done.2 = f32[8,32,256]{2,1,0:T(8,128)S(1)} async-done(((f32[8,32,256]{2,1,0:T(8,128)}), f32[8,32,256]{2,1,0:T(8,128)S(1)}, u32[]{:S(2)}, u32[]{:S(2)}) %all-to-all-start.2) | async-done | bytes 262176 | tf_op jit(solution)/shard_map/all_to_all | solution.py:136
  149.3 2.9 %convolution_bitcast_fusion.8 = f32[3072,128]{0,1:T(8,128)} fusion(bf16[256,3072]{1,0:T(8,128)(2,1)} %all-gather.2.cloned.1.call-done, bf16[256,256]{0,1:T(8,128)(2,1)S(1)} %add_convert_fusion), kind=kOutput, calls=%fused_computation.89 | convolution fusion | flops 201326592 | bytes 3211264 | tf_op jit(solution)/shard_map/dot_general | solution.py:153
  154.3 1.4 reshape.213
  157.2 58.9 %reduce-scatter.2.cloned.1.call-done = f32[384,128]{0,1:T(8,128)} async-done(((f32[3072,128]{0,1:T(8,128)}), f32[384,128]{0,1:T(8,128)}) %reduce-scatter.2.cloned.1.call-update) | async-done | bytes 196624 | tf_op jit(solution)/shard_map/reduce_scatter | solution.py:152
  216.1 1.7 copy.125
  (206 shorter events, 55.8 us)
Async XLA Ops:
  7.2 23.5 %copy-start.7 = (bf16[256,128]{1,0:T(8,128)(2,1)S(1)}, bf16[256,128]{1,0:T(8,128)(2,1)}, u32[]{:S(2)}) copy-start(bf16[256,128]{1,0:T(8,128)(2,1)} %param.11) | copy-start | bytes 196612
  7.2 24.2 %copy-start.5 = (bf16[256,768]{1,0:T(8,128)(2,1)S(1)}, bf16[256,768]{1,0:T(8,128)(2,1)}, u32[]{:S(2)}) copy-start(bf16[256,768]{1,0:T(8,128)(2,1)} %param.9) | copy-start | bytes 1179652
  9.3 13.7 %all-to-all-start = ((s32[8,1,1]{2,1,0:T(1,128)}), s32[8,1,1]{2,1,0:T(1,128)S(1)}, u32[]{:S(2)}, u32[]{:S(2)}) async-start(s32[8,1,1]{2,1,0:T(1,128)} %copy.110), calls=%async_computation | async-start | bytes 8192 | tf_op jit(solution)/shard_map/all_to_all | solution.py:30
  24.9 12.0 %all-to-all-start.1 = ((bf16[8,32,256]{2,1,0:T(8,128)(2,1)}), bf16[8,32,256]{2,1,0:T(8,128)(2,1)S(1)}, u32[]{:S(2)}, u32[]{:S(2)}) async-start(bf16[8,32,256]{2,1,0:T(8,128)(2,1)} %broadcast_select_fusion), calls=%async_computation.1 | async-start | bytes 262144 | tf_op jit(solution)/shard_map/all_to_all | solution.py:37
  28.3 120.9 %all-gather.2.cloned.1.call-start = ((), (), s32[]{:S(2)}) async-start(), calls=%async_computation.4 | async-start | bytes 1966080 | tf_op jit(solution)/shard_map/all_gather | solution.py:151
  31.4 1.8 copy-start.6
  33.2 1.8 copy-start.10
  36.9 2.3 %copy-start.8 = (f32[4,64,2,6]{1,0,3,2:T(4,128)}, f32[4,64,2,6]{1,0,3,2:T(4,128)S(1)}, u32[]{:S(2)}) copy-start(f32[4,64,2,6]{1,0,3,2:T(4,128)S(1)} %get-tuple-element.488) | copy-start | bytes 36868 | tf_op jit(solution)/shard_map/while
  36.9 4.2 %copy-start.11 = (s32[4]{0:T(128)}, s32[4]{0:T(128)S(1)}, u32[]{:S(2)}) copy-start(s32[4]{0:T(128)S(1)} %get-tuple-element.490) | copy-start | bytes 52 | tf_op jit(solution)/shard_map/while
  38.3 2.3 %copy-start.1 = (bf16[512,1,2,64]{0,3,2,1:T(8,128)(2,1)}, bf16[512,1,2,64]{0,3,2,1:T(8,128)(2,1)S(1)}, u32[]{:S(2)}) copy-start(bf16[512,1,2,64]{0,3,2,1:T(8,128)(2,1)S(1)} %copy.168) | copy-start | bytes 393220 | tf_op jit(solution)/shard_map/while
  51.9 1.0 copy-start
  53.6 4.3 %copy-start.2 = (bf16[512,1,2,64]{0,3,2,1:T(8,128)(2,1)S(1)}, bf16[512,1,2,64]{0,3,2,1:T(8,128)(2,1)}, u32[]{:S(2)}) copy-start(bf16[512,1,2,64]{0,3,2,1:T(8,128)(2,1)} %copy-done.1) | copy-start | bytes 393220 | tf_op jit(solution)/shard_map/while
  57.2 3.1 %copy-start.9 = (f32[4,64,2,6]{1,0,3,2:T(4,128)S(1)}, f32[4,64,2,6]{1,0,3,2:T(4,128)}, u32[]{:S(2)}) copy-start(f32[4,64,2,6]{1,0,3,2:T(4,128)} %copy-done.8) | copy-start | bytes 36868 | tf_op jit(solution)/shard_map/while
  57.2 3.1 %copy-start.12 = (s32[4]{0:T(128)S(1)}, s32[4]{0:T(128)}, u32[]{:S(2)}) copy-start(s32[4]{0:T(128)} %copy-done.11) | copy-start | bytes 52 | tf_op jit(solution)/shard_map/while
  60.3 2.3 %copy-start.8 = (f32[4,64,2,6]{1,0,3,2:T(4,128)}, f32[4,64,2,6]{1,0,3,2:T(4,128)S(1)}, u32[]{:S(2)}) copy-start(f32[4,64,2,6]{1,0,3,2:T(4,128)S(1)} %get-tuple-element.488) | copy-start | bytes 36868 | tf_op jit(solution)/shard_map/while
  60.3 4.1 %copy-start.11 = (s32[4]{0:T(128)}, s32[4]{0:T(128)S(1)}, u32[]{:S(2)}) copy-start(s32[4]{0:T(128)S(1)} %get-tuple-element.490) | copy-start | bytes 52 | tf_op jit(solution)/shard_map/while
  61.7 2.2 copy-start.1
  75.1 1.0 copy-start
  76.9 4.3 %copy-start.2 = (bf16[512,1,2,64]{0,3,2,1:T(8,128)(2,1)S(1)}, bf16[512,1,2,64]{0,3,2,1:T(8,128)(2,1)}, u32[]{:S(2)}) copy-start(bf16[512,1,2,64]{0,3,2,1:T(8,128)(2,1)} %copy-done.1) | copy-start | bytes 393220 | tf_op jit(solution)/shard_map/while
  80.5 3.1 %copy-start.9 = (f32[4,64,2,6]{1,0,3,2:T(4,128)S(1)}, f32[4,64,2,6]{1,0,3,2:T(4,128)}, u32[]{:S(2)}) copy-start(f32[4,64,2,6]{1,0,3,2:T(4,128)} %copy-done.8) | copy-start | bytes 36868 | tf_op jit(solution)/shard_map/while
  80.5 3.1 %copy-start.12 = (s32[4]{0:T(128)S(1)}, s32[4]{0:T(128)}, u32[]{:S(2)}) copy-start(s32[4]{0:T(128)} %copy-done.11) | copy-start | bytes 52 | tf_op jit(solution)/shard_map/while
  83.5 2.3 %copy-start.8 = (f32[4,64,2,6]{1,0,3,2:T(4,128)}, f32[4,64,2,6]{1,0,3,2:T(4,128)S(1)}, u32[]{:S(2)}) copy-start(f32[4,64,2,6]{1,0,3,2:T(4,128)S(1)} %get-tuple-element.488) | copy-start | bytes 36868 | tf_op jit(solution)/shard_map/while
  83.5 4.1 %copy-start.11 = (s32[4]{0:T(128)}, s32[4]{0:T(128)S(1)}, u32[]{:S(2)}) copy-start(s32[4]{0:T(128)S(1)} %get-tuple-element.490) | copy-start | bytes 52 | tf_op jit(solution)/shard_map/while
  84.9 2.2 copy-start.1
  98.4 1.0 copy-start
  100.2 4.3 %copy-start.2 = (bf16[512,1,2,64]{0,3,2,1:T(8,128)(2,1)S(1)}, bf16[512,1,2,64]{0,3,2,1:T(8,128)(2,1)}, u32[]{:S(2)}) copy-start(bf16[512,1,2,64]{0,3,2,1:T(8,128)(2,1)} %copy-done.1) | copy-start | bytes 393220 | tf_op jit(solution)/shard_map/while
  103.8 3.1 %copy-start.9 = (f32[4,64,2,6]{1,0,3,2:T(4,128)S(1)}, f32[4,64,2,6]{1,0,3,2:T(4,128)}, u32[]{:S(2)}) copy-start(f32[4,64,2,6]{1,0,3,2:T(4,128)} %copy-done.8) | copy-start | bytes 36868 | tf_op jit(solution)/shard_map/while
  103.8 3.1 %copy-start.12 = (s32[4]{0:T(128)S(1)}, s32[4]{0:T(128)}, u32[]{:S(2)}) copy-start(s32[4]{0:T(128)} %copy-done.11) | copy-start | bytes 52 | tf_op jit(solution)/shard_map/while
  106.9 2.3 %copy-start.8 = (f32[4,64,2,6]{1,0,3,2:T(4,128)}, f32[4,64,2,6]{1,0,3,2:T(4,128)S(1)}, u32[]{:S(2)}) copy-start(f32[4,64,2,6]{1,0,3,2:T(4,128)S(1)} %get-tuple-element.488) | copy-start | bytes 36868 | tf_op jit(solution)/shard_map/while
  106.9 4.1 %copy-start.11 = (s32[4]{0:T(128)}, s32[4]{0:T(128)S(1)}, u32[]{:S(2)}) copy-start(s32[4]{0:T(128)S(1)} %get-tuple-element.490) | copy-start | bytes 52 | tf_op jit(solution)/shard_map/while
  108.2 2.2 copy-start.1
  121.7 1.0 copy-start
  123.5 4.3 %copy-start.2 = (bf16[512,1,2,64]{0,3,2,1:T(8,128)(2,1)S(1)}, bf16[512,1,2,64]{0,3,2,1:T(8,128)(2,1)}, u32[]{:S(2)}) copy-start(bf16[512,1,2,64]{0,3,2,1:T(8,128)(2,1)} %copy-done.1) | copy-start | bytes 393220 | tf_op jit(solution)/shard_map/while
  127.0 3.1 %copy-start.9 = (f32[4,64,2,6]{1,0,3,2:T(4,128)S(1)}, f32[4,64,2,6]{1,0,3,2:T(4,128)}, u32[]{:S(2)}) copy-start(f32[4,64,2,6]{1,0,3,2:T(4,128)} %copy-done.8) | copy-start | bytes 36868 | tf_op jit(solution)/shard_map/while
  127.0 3.1 %copy-start.12 = (s32[4]{0:T(128)S(1)}, s32[4]{0:T(128)}, u32[]{:S(2)}) copy-start(s32[4]{0:T(128)} %copy-done.11) | copy-start | bytes 52 | tf_op jit(solution)/shard_map/while
  130.1 10.5 %copy-start.3 = (f32[4,256,256]{1,2,0:T(8,128)S(1)}, f32[4,256,256]{1,2,0:T(8,128)}, u32[]{:S(2)}) copy-start(f32[4,256,256]{1,2,0:T(8,128)} %get-tuple-element.178) | copy-start | bytes 3145732
  134.5 14.1 %all-to-all-start.2 = ((f32[8,32,256]{2,1,0:T(8,128)}), f32[8,32,256]{2,1,0:T(8,128)S(1)}, u32[]{:S(2)}, u32[]{:S(2)}) async-start(f32[8,32,256]{2,1,0:T(8,128)} %copy.120), calls=%async_computation.2 | async-start | bytes 524288 | tf_op jit(solution)/shard_map/all_to_all | solution.py:136
  140.4 75.8 %reduce-scatter.2.cloned.1.call-start = ((), (), s32[]{:S(2)}) async-start(), calls=%async_computation.5 | async-start | bytes 1769472 | tf_op jit(solution)/shard_map/reduce_scatter | solution.py:152
  152.2 1.1 copy-start.4
Sparse Core Ops, SparseCore 0:
  30.7 20.9 all-gather.1
  152.3 63.7 reduce-scatter.1
where the time goes:
time: 227 us; the launch traced here: 225 us
  waiting for transfers between devices  73.1 us (32%)
  matrix products  62.1 us (27%)
  local copies, waits for them, and re-layouts  44.4 us (20%)
  starting transfers between devices  16.9 us (7%)
  between operations  14.2 us (6%)
  other arithmetic  10.4 us (5%)
  loops' own time  3.57 us (2%)
    reduce_scatter x1, waiting for transfers between devices, per_device(): lax.psum_scatter(lax.dot_general(full_input, key_grad, (((0,), (0,)), (()...  58.9 us
    unnamed x22, local copies, waits for them, and re-layouts  11.4 us
    reshape x4, local copies, waits for them, and re-layouts, one_block(): key_sel_grad.reshape(NSEL, KB, half_width)  8.17 us
    all_to_all x1, waiting for transfers between devices, per_device(): lax.all_to_all(per_owner.reshape(axis_count, KB, pair_width), 'kv', split...  7.9 us
    dot_general x4, matrix products, one_block(): jnp.einsum('qhgk,khd->qhgd', slope_own, key_own, preferred_element_type=j...  7.34 us
    all_to_all x1, starting transfers between devices, per_device(): lax.all_to_all(wanted[:, None], 'kv', split_axis=0, concat_axis=0, tiled=...  7.31 us
    dynamic_update_slice x8, other arithmetic, per_device(): lax.map(one_block, (query_parts, grad_parts, sum_parts, slot_owner, usabl...  6.22 us
    all_to_all x1, starting transfers between devices, per_device(): lax.all_to_all(per_owner.reshape(axis_count, KB, pair_width), 'kv', split...  5.91 us
  transfers between devices with their start and end apart: 5, of which 3 were waited for; matrix products, arithmetic and copies ran while one was open for 47% of the time, Pallas kernels for 0%

commit v1 on v0

--- a/solution.py
+++ b/solution.py
@@ -7,6 +7,28 @@
 KB = 32
 QB = 64
 NSEL = 16
+
+
+def cut_along(x, dim, size):
+    before, after = (x.shape[:dim], x.shape[dim + 1 :])
+    return jnp.moveaxis(x.reshape(*before, size, -1, *after), dim, 0)
+
+
+def joined_along(pieces, dim):
+    pieces = jnp.moveaxis(pieces, 0, dim)
+    shape = pieces.shape
+    return pieces.reshape(*shape[:dim], shape[dim] * shape[dim + 1], *shape[dim + 2 :])
+
+
+def exchange_in_pairs(array, axis, split_dim, concat_dim):
+    peers, index = (lax.axis_size(axis), lax.axis_index(axis))
+    blocks = cut_along(array, split_dim, peers)
+    outs = [blocks[index]]
+    for turn in range(1, peers):
+        sent = blocks[index ^ turn]
+        outs.append(lax.ppermute(sent, axis, [(i, i ^ turn) for i in range(peers)]))
+    blocks = jnp.stack(outs)[index ^ jnp.arange(peers)]
+    return joined_along(blocks, concat_dim)
 
 
 def per_device(queries, key_vectors, value_vectors, log_sums, out_grad, layer_input, chosen):
@@ -27,7 +49,7 @@
     within = chosen - chosen // blocks_here * blocks_here
     matched = owner_of[:, :, None] == owners[None, None, :]
     wanted = jnp.max(jnp.where(matched, within[:, :, None], -1), axis=(0, 1))
-    incoming = lax.all_to_all(wanted[:, None], "kv", split_axis=0, concat_axis=0, tiled=True)[:, 0]
+    incoming = exchange_in_pairs(wanted[:, None], "kv", 0, 0)[:, 0]
     blocks = paired.reshape(blocks_here, KB, pair_width)
     outgoing = jnp.where(
         (incoming >= 0)[:, None, None],

time: 227 us -> 236 us (1.040)
  local copies, waits for them, and re-layouts: 44.4 us -> 49.7 us
  starting transfers between devices: 16.9 us -> 22.2 us
    ppermute x0 -> x7, starting transfers between devices: none -> 12.4 us  [exchange_in_pairs(): outs.append(lax.ppermute(sent, axis, [(i, i ^ turn) for i in range(peers)]))]
    all_to_all x1 -> x0, starting transfers between devices: 7.31 us -> none  [per_device(): lax.all_to_all(wanted[:, None], 'kv', split_axis=0, concat_axis=0, tiled=...]
    all_to_all x1 -> x0, waiting for transfers between devices: 5.53 us -> none  [per_device(): lax.all_to_all(wanted[:, None], 'kv', split_axis=0, concat_axis=0, tiled=...]
    another operation x0 -> x1, local copies, waits for them, and re-layouts: none -> 5.27 us  [exchange_in_pairs(): blocks = jnp.stack(outs)[index ^ jnp.arange(peers)]]
    ppermute x0 -> x7, waiting for transfers between devices: none -> 4.53 us  [exchange_in_pairs(): outs.append(lax.ppermute(sent, axis, [(i, i ^ turn) for i in range(peers)]))]
    unnamed x22 -> x24, local copies, waits for them, and re-layouts: 11.4 us -> 10.5 us
  transfers between devices with their start and end apart: 5 -> 11, of which waited for: 3 -> 5; matrix products, arithmetic and copies ran while one was open for 47% -> 45% of each run, Pallas kernels for 0% -> 0%
where the time goes in v1:
time: 236 us; the launch traced here: 234 us
  waiting for transfers between devices  72 us (31%)
  matrix products  62.1 us (26%)
  local copies, waits for them, and re-layouts  49.7 us (21%)
  starting transfers between devices  22.2 us (9%)
  between operations  14.3 us (6%)
  other arithmetic  9.91 us (4%)
  loops' own time  3.57 us (2%)
    reduce_scatter x1, waiting for transfers between devices, per_device(): lax.psum_scatter(lax.dot_general(full_input, key_grad, (((0,), (0,)), (()...  58.9 us
    ppermute x7, starting transfers between devices, exchange_in_pairs(): outs.append(lax.ppermute(sent, axis, [(i, i ^ turn) for i in range(peers)]))  12.4 us
    unnamed x24, local copies, waits for them, and re-layouts  10.5 us
    reshape x4, local copies, waits for them, and re-layouts, one_block(): key_sel_grad.reshape(NSEL, KB, half_width)  8.19 us
    all_to_all x1, waiting for transfers between devices, per_device(): lax.all_to_all(per_owner.reshape(axis_count, KB, pair_width), 'kv', split...  7.9 us
    dot_general x4, matrix products, one_block(): jnp.einsum('qhgk,khd->qhgd', slope_own, key_own, preferred_element_type=j...  7.41 us
    dynamic_update_slice x8, other arithmetic, per_device(): lax.map(one_block, (query_parts, grad_parts, sum_parts, slot_owner, usabl...  6.28 us
    all_to_all x1, starting transfers between devices, per_device(): lax.all_to_all(per_owner.reshape(axis_count, KB, pair_width), 'kv', split...  5.96 us
  transfers between devices with their start and end apart: 11, of which 5 were waited for; matrix products, arithmetic and copies ran while one was open for 45% of the time, Pallas kernels for 0%

profile of v1, /device:TPU:0, one launch (start us, length us, event | category | flops | bytes accessed | tf_op | source)
XLA Modules:
  0.0 233.8 jit_solution(14263770835586245475)
XLA Ops:
  7.2 1.3 broadcast_clamp_fusion
  9.4 5.0 %collective-permute-start.4 = (s32[1,1]{1,0:T(1,128)}, s32[1,1]{1,0:T(1,128)}, u32[]{:S(2)}, u32[]{:S(2)}) collective-permute-start(s32[1,1]{1,0:T(1,128)} %bitcast.9), channel_id=1, source_target_pairs={{0,20},{4,16},{8,28},{12,24},{16,4},{20,0},{24,12},{28,8},{1,21},{... | collective-permute-start | bytes 20 | tf_op jit(solution)/shard_map/ppermute | solution.py:29
  14.4 1.3 collective-permute-start.5
  15.7 2.4 %collective-permute-start.6 = (s32[1,1]{1,0:T(1,128)}, s32[1,1]{1,0:T(1,128)}, u32[]{:S(2)}, u32[]{:S(2)}) collective-permute-start(s32[1,1]{1,0:T(1,128)} %bitcast.13), channel_id=1, source_target_pairs={{0,28},{4,24},{8,20},{12,16},{16,12},{20,8},{24,4},{28,0},{1,29},{... | collective-permute-start | bytes 20 | tf_op jit(solution)/shard_map/ppermute | solution.py:29
  18.1 1.5 collective-permute-start
  20.6 2.0 collective-permute-start.2
  23.4 1.7 collective-permute-done.2
  25.1 2.0 collective-permute-done.3
  27.2 5.3 %stack.31 = s32[8,1,1]{0,2,1:T(1,128)S(1)} concatenate(s32[1,1,1]{0,2,1:T(1,128)} %bitcast, s32[1,1,1]{0,2,1:T(1,128)} %bitcast.2, s32[1,1,1]{0,2,1:T(1,128)} %bitcast.4, s32[1,1,1]{0,2,1:T(1,128)} %bitcast.6, s32[1,1,1]{0,2,1:T(1,128)} %bitcast.8, s32[1,1,1]{0,2,1:T(1,128)} %bitcast.10, s32[1,1,1]{0,2,1:T(1,128)} %bitcast.12, s32[1,1,1]{0,2,1:T(1,128)} %bitcast.14), dimensions={0} | concatenate | bytes 64 | tf_op jit(solution)/shard_map/stack | solution.py:30
  34.4 3.6 %all-to-all-start = ((bf16[8,32,256]{2,1,0:T(8,128)(2,1)}), bf16[8,32,256]{2,1,0:T(8,128)(2,1)S(1)}, u32[]{:S(2)}, u32[]{:S(2)}) async-start(bf16[8,32,256]{2,1,0:T(8,128)(2,1)} %broadcast_select_fusion), calls=%async_computation | async-start | bytes 262144 | tf_op jit(solution)/shard_map/all_to_all | solution.py:59
  43.9 1.3 and.19
  45.9 93.4 %while.18 = (s32[]{:T(128)}, bf16[4,64,2,6,64]{1,4,3,2,0:T(8,128)(2,1)}, f32[4,16,32,256]{3,2,1,0:T(8,128)}, f32[4,256,256]{1,2,0:T(8,128)}, s32[4,16]{1,0:T(4,1...) while((s32[]{:T(128)}, ...), condition=%wide.region_3.4_spmd.clone.clone, body=%wide.region_1.3_spmd.clone.clone.sunk | while | flops 458359424 | bytes 25241412 | solution.py:145
  48.2 1.4 fusion.154
  52.7 1.3 fusion.156
  54.0 1.3 fusion.157
  55.3 1.2 fusion.160
  57.5 2.1 reshape.270
  59.5 1.2 convolution_bitcast_fusion.14
  62.6 1.2 fusion.158
  67.4 1.8 fusion.159
  71.5 1.4 fusion.154
  76.0 1.3 fusion.156
  77.3 1.3 fusion.157
  78.6 1.2 fusion.160
  80.8 2.0 reshape.270
  90.7 1.9 fusion.159
  94.9 1.4 fusion.154
  98.1 1.2 fusion.155
  99.3 1.3 fusion.156
  100.6 1.3 fusion.157
  101.9 1.2 fusion.160
  104.2 2.0 reshape.270
  114.0 1.9 fusion.159
  118.2 1.4 fusion.154
  121.4 1.2 fusion.155
  122.7 1.3 fusion.156
  124.0 1.3 fusion.157
  125.3 1.2 fusion.160
  127.5 2.0 reshape.270
  132.6 1.2 fusion.158
  137.4 1.8 fusion.159
  139.3 3.5 %fusion.66 = f32[8,32,256]{2,0,1:T(8,128)S(1)} fusion(s32[64]{0:T(128)} %eq.48, pred[64]{0:T(512)(128)(4,1)} %and.19, f32[8,8,32,256]{3,2,1,0:T(8,128)} %bitcast.292), kind=kOutput, calls=%fused_computation.91 | convolution fusion | flops 50332672 | bytes 2359616 | tf_op jit(solution)/shard_map/so,sr->or/dot_general | solution.py:152
  143.6 6.0 %all-to-all-start.1 = ((f32[8,32,256]{2,1,0:T(8,128)}), f32[8,32,256]{2,1,0:T(8,128)S(1)}, u32[]{:S(2)}, u32[]{:S(2)}) async-start(f32[8,32,256]{2,1,0:T(8,128)} %copy.91), calls=%async_computation.1 | async-start | bytes 524288 | tf_op jit(solution)/shard_map/all_to_all | solution.py:158
  149.9 7.9 %all-to-all-done.1 = f32[8,32,256]{2,1,0:T(8,128)S(1)} async-done(((f32[8,32,256]{2,1,0:T(8,128)}), f32[8,32,256]{2,1,0:T(8,128)S(1)}, u32[]{:S(2)}, u32[]{:S(2)}) %all-to-all-start.1) | async-done | bytes 262176 | tf_op jit(solution)/shard_map/all_to_all | solution.py:158
  158.4 2.9 %convolution_bitcast_fusion.8 = f32[3072,128]{0,1:T(8,128)} fusion(bf16[256,3072]{1,0:T(8,128)(2,1)} %all-gather.2.cloned.1.call-done, bf16[256,256]{0,1:T(8,128)(2,1)S(1)} %add_convert_fusion), kind=kOutput, calls=%fused_computation.90 | convolution fusion | flops 201326592 | bytes 3211264 | tf_op jit(solution)/shard_map/dot_general | solution.py:175
  163.5 1.4 reshape.260
  166.3 58.9 %reduce-scatter.2.cloned.1.call-done = f32[384,128]{0,1:T(8,128)} async-done(((f32[3072,128]{0,1:T(8,128)}), f32[384,128]{0,1:T(8,128)}) %reduce-scatter.2.cloned.1.call-update) | async-done | bytes 196624 | tf_op jit(solution)/shard_map/reduce_scatter | solution.py:174
  225.2 1.7 copy.96
  (224 shorter events, 63.6 us)
Async XLA Ops:
  7.2 31.6 %copy-start.7 = (bf16[256,128]{1,0:T(8,128)(2,1)S(1)}, bf16[256,128]{1,0:T(8,128)(2,1)}, u32[]{:S(2)}) copy-start(bf16[256,128]{1,0:T(8,128)(2,1)} %param.10) | copy-start | bytes 196612
  7.2 32.3 %copy-start.8 = (bf16[256,128]{1,0:T(8,128)(2,1)S(1)}, bf16[256,128]{1,0:T(8,128)(2,1)}, u32[]{:S(2)}) copy-start(bf16[256,128]{1,0:T(8,128)(2,1)} %param.11) | copy-start | bytes 196612
  7.2 33.1 %copy-start.5 = (bf16[256,768]{1,0:T(8,128)(2,1)S(1)}, bf16[256,768]{1,0:T(8,128)(2,1)}, u32[]{:S(2)}) copy-start(bf16[256,768]{1,0:T(8,128)(2,1)} %param.9) | copy-start | bytes 1179652
  9.4 11.2 %collective-permute-start.4 = (s32[1,1]{1,0:T(1,128)}, s32[1,1]{1,0:T(1,128)}, u32[]{:S(2)}, u32[]{:S(2)}) collective-permute-start(s32[1,1]{1,0:T(1,128)} %bitcast.9), channel_id=1, source_target_pairs={{0,20},{4,16},{8,28},{12,24},{16,4},{20,0},{24,12},{28,8},{1,21},{... | collective-permute-start | bytes 20 | tf_op jit(solution)/shard_map/ppermute | solution.py:29
  14.4 8.2 %collective-permute-start.5 = (s32[1,1]{1,0:T(1,128)}, s32[1,1]{1,0:T(1,128)}, u32[]{:S(2)}, u32[]{:S(2)}) collective-permute-start(s32[1,1]{1,0:T(1,128)} %bitcast.11), channel_id=1, source_target_pairs={{0,24},{4,28},{8,16},{12,20},{16,8},{20,12},{24,0},{28,4},{1,25},{... | collective-permute-start | bytes 20 | tf_op jit(solution)/shard_map/ppermute | solution.py:29
  15.7 6.9 %collective-permute-start.6 = (s32[1,1]{1,0:T(1,128)}, s32[1,1]{1,0:T(1,128)}, u32[]{:S(2)}, u32[]{:S(2)}) collective-permute-start(s32[1,1]{1,0:T(1,128)} %bitcast.13), channel_id=1, source_target_pairs={{0,28},{4,24},{8,20},{12,16},{16,12},{20,8},{24,4},{28,0},{1,29},{... | collective-permute-start | bytes 20 | tf_op jit(solution)/shard_map/ppermute | solution.py:29
  18.1 4.5 %collective-permute-start = (s32[1,1]{1,0:T(1,128)}, s32[1,1]{1,0:T(1,128)}, u32[]{:S(2)}, u32[]{:S(2)}) collective-permute-start(s32[1,1]{1,0:T(1,128)} %bitcast.1), channel_id=1, source_target_pairs={{0,4},{4,0},{8,12},{12,8},{16,20},{20,16},{24,28},{28,24},{1,5},{5... | collective-permute-start | bytes 20 | tf_op jit(solution)/shard_map/ppermute | solution.py:29
  19.7 3.7 %collective-permute-start.1 = (s32[1,1]{1,0:T(1,128)}, s32[1,1]{1,0:T(1,128)}, u32[]{:S(2)}, u32[]{:S(2)}) collective-permute-start(s32[1,1]{1,0:T(1,128)} %bitcast.3), channel_id=1, source_target_pairs={{0,8},{4,12},{8,0},{12,4},{16,24},{20,28},{24,16},{28,20},{1,9},{5... | collective-permute-start | bytes 20 | tf_op jit(solution)/shard_map/ppermute | solution.py:29
  20.6 4.5 %collective-permute-start.2 = (s32[1,1]{1,0:T(1,128)}, s32[1,1]{1,0:T(1,128)}, u32[]{:S(2)}, u32[]{:S(2)}) collective-permute-start(s32[1,1]{1,0:T(1,128)} %bitcast.5), channel_id=1, source_target_pairs={{0,12},{4,8},{8,4},{12,0},{16,28},{20,24},{24,20},{28,16},{1,13},{... | collective-permute-start | bytes 20 | tf_op jit(solution)/shard_map/ppermute | solution.py:29
  22.6 4.6 %collective-permute-start.3 = (s32[1,1]{1,0:T(1,128)}, s32[1,1]{1,0:T(1,128)}, u32[]{:S(2)}, u32[]{:S(2)}) collective-permute-start(s32[1,1]{1,0:T(1,128)} %bitcast.7), channel_id=1, source_target_pairs={{0,16},{4,20},{8,24},{12,28},{16,0},{20,4},{24,8},{28,12},{1,17},{... | collective-permute-start | bytes 20 | tf_op jit(solution)/shard_map/ppermute | solution.py:29
  34.4 11.5 %all-to-all-start = ((bf16[8,32,256]{2,1,0:T(8,128)(2,1)}), bf16[8,32,256]{2,1,0:T(8,128)(2,1)S(1)}, u32[]{:S(2)}, u32[]{:S(2)}) async-start(bf16[8,32,256]{2,1,0:T(8,128)(2,1)} %broadcast_select_fusion), calls=%async_computation | async-start | bytes 262144 | tf_op jit(solution)/shard_map/all_to_all | solution.py:59
  38.0 120.4 %all-gather.2.cloned.1.call-start = ((), (), s32[]{:S(2)}) async-start(), calls=%async_computation.3 | async-start | bytes 1966080 | tf_op jit(solution)/shard_map/all_gather | solution.py:173
  40.3 1.8 copy-start.6
  42.0 1.8 copy-start.11
  45.9 2.3 copy-start.9
  45.9 4.2 %copy-start.12 = (s32[4]{0:T(128)}, s32[4]{0:T(128)S(1)}, u32[]{:S(2)}) copy-start(s32[4]{0:T(128)S(1)} %get-tuple-element.478) | copy-start | bytes 52 | tf_op jit(solution)/shard_map/while
  47.3 2.3 copy-start.1
  60.8 1.0 copy-start
  62.6 4.3 %copy-start.2 = (bf16[512,1,2,64]{0,3,2,1:T(8,128)(2,1)S(1)}, bf16[512,1,2,64]{0,3,2,1:T(8,128)(2,1)}, u32[]{:S(2)}) copy-start(bf16[512,1,2,64]{0,3,2,1:T(8,128)(2,1)} %copy-done.1) | copy-start | bytes 393220 | tf_op jit(solution)/shard_map/while
  66.2 3.1 %copy-start.10 = (f32[4,64,2,6]{1,0,3,2:T(4,128)S(1)}, f32[4,64,2,6]{1,0,3,2:T(4,128)}, u32[]{:S(2)}) copy-start(f32[4,64,2,6]{1,0,3,2:T(4,128)} %copy-done.9) | copy-start | bytes 36868 | tf_op jit(solution)/shard_map/while
  66.2 3.1 %copy-start.13 = (s32[4]{0:T(128)S(1)}, s32[4]{0:T(128)}, u32[]{:S(2)}) copy-start(s32[4]{0:T(128)} %copy-done.12) | copy-start | bytes 52 | tf_op jit(solution)/shard_map/while
  69.2 2.3 copy-start.9
  69.2 4.2 %copy-start.12 = (s32[4]{0:T(128)}, s32[4]{0:T(128)S(1)}, u32[]{:S(2)}) copy-start(s32[4]{0:T(128)S(1)} %get-tuple-element.478) | copy-start | bytes 52 | tf_op jit(solution)/shard_map/while
  70.6 2.3 copy-start.1
  84.1 1.0 copy-start
  85.9 4.3 %copy-start.2 = (bf16[512,1,2,64]{0,3,2,1:T(8,128)(2,1)S(1)}, bf16[512,1,2,64]{0,3,2,1:T(8,128)(2,1)}, u32[]{:S(2)}) copy-start(bf16[512,1,2,64]{0,3,2,1:T(8,128)(2,1)} %copy-done.1) | copy-start | bytes 393220 | tf_op jit(solution)/shard_map/while
  89.5 3.1 %copy-start.10 = (f32[4,64,2,6]{1,0,3,2:T(4,128)S(1)}, f32[4,64,2,6]{1,0,3,2:T(4,128)}, u32[]{:S(2)}) copy-start(f32[4,64,2,6]{1,0,3,2:T(4,128)} %copy-done.9) | copy-start | bytes 36868 | tf_op jit(solution)/shard_map/while
  89.5 3.1 %copy-start.13 = (s32[4]{0:T(128)S(1)}, s32[4]{0:T(128)}, u32[]{:S(2)}) copy-start(s32[4]{0:T(128)} %copy-done.12) | copy-start | bytes 52 | tf_op jit(solution)/shard_map/while
  92.6 2.3 copy-start.9
  92.6 4.2 %copy-start.12 = (s32[4]{0:T(128)}, s32[4]{0:T(128)S(1)}, u32[]{:S(2)}) copy-start(s32[4]{0:T(128)S(1)} %get-tuple-element.478) | copy-start | bytes 52 | tf_op jit(solution)/shard_map/while
  94.0 2.3 copy-start.1
  107.4 1.0 copy-start
  109.2 4.3 %copy-start.2 = (bf16[512,1,2,64]{0,3,2,1:T(8,128)(2,1)S(1)}, bf16[512,1,2,64]{0,3,2,1:T(8,128)(2,1)}, u32[]{:S(2)}) copy-start(bf16[512,1,2,64]{0,3,2,1:T(8,128)(2,1)} %copy-done.1) | copy-start | bytes 393220 | tf_op jit(solution)/shard_map/while
  112.8 3.1 %copy-start.10 = (f32[4,64,2,6]{1,0,3,2:T(4,128)S(1)}, f32[4,64,2,6]{1,0,3,2:T(4,128)}, u32[]{:S(2)}) copy-start(f32[4,64,2,6]{1,0,3,2:T(4,128)} %copy-done.9) | copy-start | bytes 36868 | tf_op jit(solution)/shard_map/while
  112.8 3.1 %copy-start.13 = (s32[4]{0:T(128)S(1)}, s32[4]{0:T(128)}, u32[]{:S(2)}) copy-start(s32[4]{0:T(128)} %copy-done.12) | copy-start | bytes 52 | tf_op jit(solution)/shard_map/while
  115.9 2.3 copy-start.9
  115.9 4.2 %copy-start.12 = (s32[4]{0:T(128)}, s32[4]{0:T(128)S(1)}, u32[]{:S(2)}) copy-start(s32[4]{0:T(128)S(1)} %get-tuple-element.478) | copy-start | bytes 52 | tf_op jit(solution)/shard_map/while
  117.3 2.3 copy-start.1
  130.8 1.0 copy-start
  132.6 4.3 %copy-start.2 = (bf16[512,1,2,64]{0,3,2,1:T(8,128)(2,1)S(1)}, bf16[512,1,2,64]{0,3,2,1:T(8,128)(2,1)}, u32[]{:S(2)}) copy-start(bf16[512,1,2,64]{0,3,2,1:T(8,128)(2,1)} %copy-done.1) | copy-start | bytes 393220 | tf_op jit(solution)/shard_map/while
  136.1 3.1 %copy-start.10 = (f32[4,64,2,6]{1,0,3,2:T(4,128)S(1)}, f32[4,64,2,6]{1,0,3,2:T(4,128)}, u32[]{:S(2)}) copy-start(f32[4,64,2,6]{1,0,3,2:T(4,128)} %copy-done.9) | copy-start | bytes 36868 | tf_op jit(solution)/shard_map/while
  136.1 3.1 %copy-start.13 = (s32[4]{0:T(128)S(1)}, s32[4]{0:T(128)}, u32[]{:S(2)}) copy-start(s32[4]{0:T(128)} %copy-done.12) | copy-start | bytes 52 | tf_op jit(solution)/shard_map/while
  139.2 10.5 %copy-start.3 = (f32[4,256,256]{1,2,0:T(8,128)S(1)}, f32[4,256,256]{1,2,0:T(8,128)}, u32[]{:S(2)}) copy-start(f32[4,256,256]{1,2,0:T(8,128)} %get-tuple-element.178) | copy-start | bytes 3145732
  143.6 14.2 %all-to-all-start.1 = ((f32[8,32,256]{2,1,0:T(8,128)}), f32[8,32,256]{2,1,0:T(8,128)S(1)}, u32[]{:S(2)}, u32[]{:S(2)}) async-start(f32[8,32,256]{2,1,0:T(8,128)} %copy.91), calls=%async_computation.1 | async-start | bytes 524288 | tf_op jit(solution)/shard_map/all_to_all | solution.py:158
  149.5 75.7 %reduce-scatter.2.cloned.1.call-start = ((), (), s32[]{:S(2)}) async-start(), calls=%async_computation.4 | async-start | bytes 1769472 | tf_op jit(solution)/shard_map/reduce_scatter | solution.py:174
  161.4 1.1 copy-start.4
Sparse Core Ops, SparseCore 0:
  40.4 21.0 all-gather.1
  161.5 63.6 reduce-scatter.1
